TPU v7x, 32 devices: a whole 2x2x4 slice. The times are simulated.
32 devices in a mesh: grp: 2 (over y), sp: 4 (over z), tp: 4 (over x, core).
Axes of the slice: x: 2, y: 2, z: 4, core: 2. Of those that a mesh axis runs over, the one named last changes fastest.
Arguments:
- stream: bfloat16 [1024, 2048], P(('grp', 'sp')), parts along dimension 0, may hold values from -40 to 40
- queries: bfloat16 [1024, 1024], P(('grp', 'sp'), 'tp'), parts along dimension 0, may hold values from -6 to 6
- key_matrix: bfloat16 [1024, 1024], P(('grp', 'sp'), 'tp'), parts along dimension 0, may hold values from -6 to 6
- value_matrix: bfloat16 [1024, 2048], P(('grp', 'sp'), 'tp'), parts along dimension 0, may hold values from -6 to 6
- output_gate_logits: bfloat16 [1024, 2048], P(('grp', 'sp'), 'tp'), parts along dimension 0, may hold values from -6 to 6
- forgetting_raw_score: float32 [1024, 1024], P(('grp', 'sp'), 'tp'), parts along dimension 0, may hold values from -2 to 12
- additional_forgetting_rate: float32 [1024, 1024], P(('grp', 'sp'), 'tp'), parts along dimension 0, may hold values from -0.7 to 0
- head_norm_gain: float32 [2048], P('tp'), may hold values from 0.1 to 1.9
- output_weight: bfloat16 [2048, 2048], P('tp'), may hold values from -0.125 to 0.125
- feedforward_norm_gain: bfloat16 [2048], replicated, may hold values from 0.099609375 to 1.8984375
- gate_weight: bfloat16 [2048, 5632], P('sp', 'tp'), may hold values from -0.125 to 0.125
- up_weight: bfloat16 [2048, 5632], P('sp', 'tp'), may hold values from -0.125 to 0.125
- down_weight: bfloat16 [5632, 2048], P('tp', 'sp'), may hold values from -0.078125 to 0.078125
Outputs:
- layer_out: bfloat16 [1024, 2048], P(('grp', 'sp'), 'tp'), parts along dimension 0
There are 2 independent parts, one for each index of `grp`. A program takes and returns all parts, laid end to end along the dimension named above; an argument that names none is the same for every part. Nothing has to cross between parts.
All inputs are finite; a program needn't handle non-finite values.
Results may differ from a plain program's by a relative error of at most 0.013.
Values may be sent and summed in bfloat16 or wider, within the bound.
A program may use at most 128 MiB of HBM per device.

v0:
```python
import jax
import jax.numpy as jnp
from jax import lax
from jax.sharding import PartitionSpec as P

HK = 256
HV = 512
BLOCK = 64


epsilon = 1e-06
sigmoid_sharpness = 16.0
highest = lax.Precision.HIGHEST


def carried_in(value, axis, join, neutral):
    place = lax.axis_index(axis)
    gathered = jax.tree.map(
        lambda a, kind: lax.all_gather(a.astype(kind), axis), value, (jnp.bfloat16, jnp.bfloat16)
    )
    state = jax.tree.map(lambda a, e: jnp.zeros_like(a) + jnp.asarray(e, a.dtype), value, neutral)

    def one(turn, state):
        return join(
            state,
            jax.tree.map(
                lambda a, own: lax.dynamic_index_in_dim(a, turn, 0, False).astype(own.dtype),
                gathered,
                value,
            ),
        )

    return lax.fori_loop(0, place, one, state)


def split_heads(tensor, blocks, count, depth):
    return tensor.astype(jnp.float32).reshape(blocks, BLOCK, count, depth).transpose(2, 0, 1, 3)


def combine(earlier, later):
    return (earlier[0] * later[0], later[0][:, :, None] * earlier[1] + later[1])


def local(
    stream,
    queries,
    key_matrix,
    value_matrix,
    output_gate_logits,
    forgetting_raw_score,
    additional_forgetting_rate,
    head_norm_gain,
    output_weight,
    feedforward_norm_gain,
    gate_weight,
    up_weight,
    down_weight,
):
    tokens = queries.shape[0]
    owned_heads = queries.shape[1] // HK
    blocks = tokens // BLOCK
    forgetting_exponent = (
        jax.nn.log_sigmoid(forgetting_raw_score) / sigmoid_sharpness + additional_forgetting_rate
    )
    query_part = split_heads(queries, blocks, owned_heads, HK) * HK ** (-0.5)
    key_part = split_heads(key_matrix, blocks, owned_heads, HK)
    value_part = split_heads(value_matrix, blocks, owned_heads, HV)
    decay_part = split_heads(forgetting_exponent, blocks, owned_heads, HK)
    within = jnp.cumsum(decay_part, axis=2)
    closing = within[:, :, -1, :]
    query_in = query_part * jnp.exp(within)
    key_in = key_part * jnp.exp(-within)
    key_end = key_part * jnp.exp(closing[:, :, None, :] - within)
    causal = jnp.tril(jnp.ones((BLOCK, BLOCK), jnp.bool_))
    scores = jnp.einsum("hntd,hnsd->hnts", query_in, key_in, precision=highest)
    scores = jnp.where(causal, scores, 0.0)
    inside = jnp.einsum("hnts,hnsv->hntv", scores, value_part, precision=highest)

    def advance(memory, inputs):
        query_block, key_block, value_block, decay_block = inputs
        final_answer = jnp.einsum("htd,hdv->htv", query_block, memory, precision=highest)
        memory = decay_block[:, :, None] * memory + jnp.einsum(
            "hsd,hsv->hdv", key_block, value_block, precision=highest
        )
        return (memory, final_answer)

    sequence = (
        jnp.moveaxis(query_in, 1, 0),
        jnp.moveaxis(key_end, 1, 0),
        jnp.moveaxis(value_part, 1, 0),
        jnp.moveaxis(jnp.exp(closing), 1, 0),
    )
    start_memory = jnp.zeros((owned_heads, HK, HV), jnp.float32)
    final_memory, earlier_blocks = lax.scan(advance, start_memory, sequence)
    device_decay = jnp.exp(jnp.sum(closing, axis=1))
    neutral = (jnp.ones_like(device_decay), jnp.zeros_like(final_memory))
    _, carried = carried_in((device_decay, final_memory), "sp", combine, neutral)
    before = jnp.cumsum(closing, axis=1) - closing
    query_far = query_in * jnp.exp(before[:, :, None, :])
    outside = jnp.einsum("hntd,hdv->hntv", query_far, carried, precision=highest)
    mixed_heads = inside + jnp.moveaxis(earlier_blocks, 0, 1) + outside
    mixed_heads = mixed_heads.transpose(1, 2, 0, 3).reshape(tokens, owned_heads, HV)
    mixed_heads = mixed_heads * lax.rsqrt(
        jnp.mean(mixed_heads * mixed_heads, axis=-1, keepdims=True) + epsilon
    )
    gated_rows = (
        mixed_heads.reshape(tokens, owned_heads * HV)
        * head_norm_gain
        * jax.nn.silu(output_gate_logits.astype(jnp.float32))
    ).astype(jnp.bfloat16)
    partial_out = jnp.dot(gated_rows, output_weight, preferred_element_type=jnp.float32)
    model_width = stream.shape[1]
    column_share = model_width // lax.axis_size("tp")
    column_start = lax.axis_index("tp") * column_share
    attn_cols = lax.psum_scatter(
        partial_out.astype(jnp.bfloat16), "tp", scatter_dimension=1, tiled=True
    ).astype(jnp.float32)
    resid_part = (
        lax.dynamic_slice_in_dim(stream, column_start, column_share, 1).astype(jnp.float32)
        + attn_cols
    )
    elementwise_power = lax.psum(jnp.sum(resid_part * resid_part, axis=1), "tp")
    gain_part = lax.dynamic_slice_in_dim(
        feedforward_norm_gain, column_start, column_share, 0
    ).astype(jnp.float32)
    rescaled_portion = (
        resid_part * lax.rsqrt(elementwise_power / model_width + epsilon)[:, None] * gain_part
    ).astype(jnp.bfloat16)
    normed = lax.all_gather(rescaled_portion, "tp", axis=1, tiled=True)
    gate_sum = jnp.dot(
        normed,
        lax.all_gather(gate_weight, "sp", axis=0, tiled=True),
        preferred_element_type=jnp.float32,
    )
    up_sum = jnp.dot(
        normed,
        lax.all_gather(up_weight, "sp", axis=0, tiled=True),
        preferred_element_type=jnp.float32,
    )
    hidden = (jax.nn.silu(gate_sum) * up_sum).astype(jnp.bfloat16)
    down_sum = jnp.dot(
        hidden,
        lax.all_gather(down_weight, "sp", axis=1, tiled=True),
        preferred_element_type=jnp.float32,
    )
    ffn_part = lax.psum_scatter(
        down_sum.astype(jnp.bfloat16), "tp", scatter_dimension=1, tiled=True
    ).astype(jnp.float32)
    return (resid_part + ffn_part).astype(jnp.bfloat16)


def solution(mesh):
    return jax.shard_map(
        local,
        mesh=mesh,
        in_specs=(
            P(("grp", "sp"), None),
            P(("grp", "sp"), "tp"),
            P(("grp", "sp"), "tp"),
            P(("grp", "sp"), "tp"),
            P(("grp", "sp"), "tp"),
            P(("grp", "sp"), "tp"),
            P(("grp", "sp"), "tp"),
            P("tp"),
            P("tp", None),
            P(),
            P("sp", "tp"),
            P("sp", "tp"),
            P("tp", "sp"),
        ),
        out_specs=P(("grp", "sp"), "tp"),
        check_vma=False,
    )
```

profile of v0, /device:TPU:0, one launch (start us, length us, event | category | flops | bytes accessed | tf_op | source)
XLA Modules:
  0.0 430.0 jit_solution(5797290989619579910)
XLA Ops:
  6.5 1.2 fusion.27
  8.0 0.9 convert_element_type.88
  8.9 0.9 convert.4
  9.8 1.5 bitcast_multiply_fusion.1
  11.4 3.6 while.26
  11.4 1.1 fusion.60
  13.2 1.1 fusion.60
  15.8 12.6 %all-gather.2 = bf16[4,1,256]{2,1,0:T(2,128)(2,1)S(1)} all-gather(bf16[1,1,256]{2,1,0:T(2,128)(2,1)S(1)} %reshape.243), channel_id=2, replica_groups=mesh['grp'=2,'sp'=4,'tp'=4] {'sp'}, dimensions={0}, use_global_device_ids=true | all-gather | bytes 2560 | tf_op jit(solution)/shard_map/all_gather | solution.py:19
  28.8 1.3 convolution_add_fusion.1
  30.1 16.3 %all-gather.14.cloned.1.call-done = bf16[4,256,512]{2,1,0:T(8,128)(2,1)} async-done(((bf16[1,256,512]{2,1,0:T(8,128)(2,1)}), bf16[4,256,512]{2,1,0:T(8,128)(2,1)}) %all-gather.14.cloned.1.call-update) | async-done | bytes 1048592 | tf_op jit(solution)/shard_map/all_gather | solution.py:19
  47.2 1.2 convolution_convert_fusion
  50.5 0.8 dynamic-slice_convert_fusion.1
  51.2 22.1 %reduce-scatter.3.cloned.1.call-done = bf16[128,512]{1,0:T(8,128)(2,1)} async-done(((bf16[128,2048]{1,0:T(8,128)(2,1)}), bf16[128,512]{1,0:T(8,128)(2,1)}) %reduce-scatter.3.cloned.1.call-update) | async-done | bytes 131088 | tf_op jit(solution)/shard_map/reduce_scatter | solution.py:115
  73.3 1.1 multiply_reduce_fusion
  74.4 5.8 %psum.7 = f32[128]{0:T(128)S(1)} all-reduce(f32[128]{0:T(128)S(1)} %multiply_reduce_fusion), channel_id=1, replica_groups=mesh['grp'=2,'sp'=4,'tp'=4] {'tp'}, use_global_device_ids=true, to_apply=%region_10.11 | all-reduce | flops 128 | bytes 1024 | tf_op jit(solution)/shard_map/psum | solution.py:122
  80.2 1.1 multiply_convert_fusion
  81.2 6.9 %all_gather.25 = bf16[128,2048]{1,0:T(8,128)(2,1)S(1)} all-gather(bf16[128,512]{1,0:T(8,128)(2,1)S(1)} %multiply_convert_fusion), channel_id=1, replica_groups=mesh['grp'=2,'sp'=4,'tp'=4] {'tp'}, dimensions={1}, use_global_device_ids=true | all-gather | bytes 655360 | tf_op jit(solution)/shard_map/all_gather | solution.py:129
  88.1 93.5 %all-gather.8.cloned.1.call-done = bf16[2048,1408]{1,0:T(8,128)(2,1)} async-done(((bf16[512,1408]{1,0:T(8,128)(2,1)}), bf16[2048,1408]{1,0:T(8,128)(2,1)}) %all-gather.8.cloned.1.call-update) | async-done | bytes 5767184 | tf_op jit(solution)/shard_map/all_gather | solution.py:132
  181.6 3.6 fusion.38
  185.3 102.8 %all-gather.10.cloned.1.call-done = bf16[2048,1408]{1,0:T(8,128)(2,1)} async-done(((bf16[512,1408]{1,0:T(8,128)(2,1)}), bf16[2048,1408]{1,0:T(8,128)(2,1)}) %all-gather.10.cloned.1.call-update) | async-done | bytes 5767184 | tf_op jit(solution)/shard_map/all_gather | solution.py:137
  288.0 106.4 %all-gather.12.cloned.1.call-done = bf16[1408,2048]{1,0:T(8,128)(2,1)} async-done(((bf16[1408,512]{1,0:T(8,128)(2,1)}), bf16[1408,2048]{1,0:T(8,128)(2,1)}) %all-gather.12.cloned.1.call-update) | async-done | bytes 5767184 | tf_op jit(solution)/shard_map/all_gather | solution.py:143
  394.4 7.0 %convolution_convert_fusion.1 = bf16[128,2048]{1,0:T(8,128)(2,1)} fusion(bf16[1408,2048]{1,0:T(8,128)(2,1)} %all-gather.12.cloned.1.call-done, bf16[128,2048]{1,0:T(8,128)(2,1)S(1)} %all_gather.25, bf16[2048,1408]{1,0:T(8,128)(2,1)} %all-gather.10.cloned.1.call-done, f32[128,1408]{1,0:T(8,128)S(1)} %fusion.38), kind=kOutput, calls=%fused_computation.23 | convolution fusion | flops 1477738496 | bytes 13303808 | tf_op jit(solution)/shard_map/dot_general | solution.py:141
  401.5 20.0 %reduce-scatter.5.cloned.1.call-done = bf16[128,512]{1,0:T(8,128)(2,1)} async-done(((bf16[128,2048]{1,0:T(8,128)(2,1)}), bf16[128,512]{1,0:T(8,128)(2,1)}) %reduce-scatter.5.cloned.1.call-update) | async-done | bytes 131088 | tf_op jit(solution)/shard_map/reduce_scatter | solution.py:146
  421.5 1.7 add_convert_fusion
  (47 shorter events, 5.5 us)
Async XLA Ops:
  6.5 40.7 %copy-start = (bf16[512,2048]{1,0:T(8,128)(2,1)S(1)}, bf16[512,2048]{1,0:T(8,128)(2,1)}, u32[]{:S(2)}) copy-start(bf16[512,2048]{1,0:T(8,128)(2,1)} %param.25) | copy-start | bytes 6291460
  6.5 39.9 %all-gather.14.cloned.1.call-start = ((), (), s32[]{:S(2)}) async-start(), calls=%async_computation.7 | async-start | bytes 1310720 | tf_op jit(solution)/shard_map/all_gather | solution.py:19
  15.0 32.1 %copy-start.4 = (f32[512]{0:T(512)S(1)}, f32[512]{0:T(512)}, u32[]{:S(2)}) copy-start(f32[512]{0:T(512)} %param.24) | copy-start | bytes 6148
  15.7 57.6 %reduce-scatter.3.cloned.1.call-start = ((), (), s32[]{:S(2)}) async-start(), calls=%async_computation.2 | async-start | bytes 655360 | tf_op jit(solution)/shard_map/reduce_scatter | solution.py:115
  28.8 17.7 %copy-start.2 = (f32[128,256]{1,0:T(8,128)S(1)}, f32[128,256]{1,0:T(8,128)}, u32[]{:S(2)}) copy-start(f32[128,256]{1,0:T(8,128)} %get-tuple-element.167) | copy-start | bytes 393220
  28.8 18.3 %copy-start.3 = (bf16[128,512]{1,0:T(8,128)(2,1)S(1)}, bf16[128,512]{1,0:T(8,128)(2,1)}, u32[]{:S(2)}) copy-start(bf16[128,512]{1,0:T(8,128)(2,1)} %param.21) | copy-start | bytes 393220
  48.5 133.1 %all-gather.8.cloned.1.call-start = ((), (), s32[]{:S(2)}) async-start(), calls=%async_computation.3 | async-start | bytes 7208960 | tf_op jit(solution)/shard_map/all_gather | solution.py:132
  49.2 238.8 %all-gather.10.cloned.1.call-start = ((), (), s32[]{:S(2)}) async-start(), calls=%async_computation.4 | async-start | bytes 7208960 | tf_op jit(solution)/shard_map/all_gather | solution.py:137
  49.8 344.6 %all-gather.12.cloned.1.call-start = ((), (), s32[]{:S(2)}) async-start(), calls=%async_computation.5 | async-start | bytes 7208960 | tf_op jit(solution)/shard_map/all_gather | solution.py:143
  50.4 371.1 %reduce-scatter.5.cloned.1.call-start = ((), (), s32[]{:S(2)}) async-start(), calls=%async_computation.6 | async-start | bytes 655360 | tf_op jit(solution)/shard_map/reduce_scatter | solution.py:146
  185.3 236.3 %copy-start.1 = (bf16[128,512]{1,0:T(8,128)(2,1)S(1)}, bf16[128,512]{1,0:T(8,128)(2,1)}, u32[]{:S(2)}) copy-start(bf16[128,512]{1,0:T(8,128)(2,1)} %reduce-scatter.3.cloned.1.call-done) | copy-start | bytes 393220
Sparse Core Ops, SparseCore 0:
  15.9 30.5 all-gather.13
  48.9 24.3 reduce-scatter.2
  74.9 106.6 all-gather.7
  183.1 104.9 all-gather.9
  289.4 104.9 all-gather.11
  401.6 19.8 reduce-scatter.4
where the time goes:
time: 431 us; the launch traced here: 430 us
  waiting for transfers between devices  363 us (84%)
  blocking collectives  25.3 us (6%)
  matrix products  17.6 us (4%)
  between operations  13.7 us (3%)
  other arithmetic  10.2 us (2%)
    all_gather x1, waiting for transfers between devices, local(): lax.all_gather(down_weight, 'sp', axis=1, tiled=True)  106 us
    all_gather x1, waiting for transfers between devices, local(): lax.all_gather(up_weight, 'sp', axis=0, tiled=True)  103 us
    all_gather x1, waiting for transfers between devices, local(): lax.all_gather(gate_weight, 'sp', axis=0, tiled=True)  93.5 us
    reduce_scatter x1, waiting for transfers between devices, local(): lax.psum_scatter(partial_out.astype(jnp.bfloat16), 'tp', scatter_dimensio...  22.1 us
    reduce_scatter x1, waiting for transfers between devices, local(): lax.psum_scatter(down_sum.astype(jnp.bfloat16), 'tp', scatter_dimension=1...  20 us
    all_gather x1, waiting for transfers between devices, carried_in(): lax.all_gather(a.astype(kind), axis)  16.3 us
    all_gather x1, blocking collectives, carried_in(): lax.all_gather(a.astype(kind), axis)  12.6 us
  transfers between devices with their start and end apart: 6, of which 6 were waited for; matrix products, arithmetic and copies ran while one was open for 2% of the time, Pallas kernels for 0%

commit v1 on v0

--- a/solution.py
+++ b/solution.py
@@ -39,6 +39,60 @@
 
 def combine(earlier, later):
     return (earlier[0] * later[0], later[0][:, :, None] * earlier[1] + later[1])
+
+
+def swap_units(weight, unit_axis):
+    places = lax.axis_size("sp")
+    copies = lax.axis_size("grp")
+    place = lax.axis_index("sp")
+    copy = lax.axis_index("grp")
+    other = 1 - unit_axis
+    units = weight.shape[unit_axis] // places
+    depth = weight.shape[other]
+    part = depth // copies
+    shape = [0, 0]
+    shape[unit_axis] = units
+    shape[other] = depth * places
+    whole = jnp.zeros(shape, weight.dtype)
+
+    def put(whole, block, at):
+        return lax.dynamic_update_slice_in_dim(whole, block, at, other)
+
+    own = lax.dynamic_slice_in_dim(weight, place * units, units, unit_axis)
+    pieces = []
+    for shift in range(1, places):
+        target = (place + shift) % places
+        block = lax.dynamic_slice_in_dim(weight, target * units, units, unit_axis)
+        block = lax.dynamic_slice_in_dim(block, copy * part, part, other)
+        ring = [(i, (i + shift) % places) for i in range(places)]
+        pieces.append((shift, lax.ppermute(block, "sp", ring)))
+    whole = put(whole, own, place * depth)
+    for shift, block in pieces:
+        source = (place - shift) % places
+        whole = put(whole, block, source * depth + copy * part)
+        for turn in range(1, copies):
+            ring = [(i, (i + turn) % copies) for i in range(copies)]
+            passed = lax.ppermute(block, "grp", ring)
+            whole = put(whole, passed, source * depth + ((copy - turn) % copies) * part)
+    return whole
+
+
+def spread_units(normed_part, gate_weight, up_weight, down_weight):
+    normed = lax.all_gather(normed_part, ("sp", "tp"))
+    places = lax.axis_size("sp")
+    shares = lax.axis_size("tp")
+    tokens, width = normed_part.shape
+    normed = normed.reshape(places, shares, tokens, width).transpose(0, 2, 1, 3)
+    normed = normed.reshape(places * tokens, shares * width)
+    gate = swap_units(gate_weight, 1)
+    up = swap_units(up_weight, 1)
+    down = swap_units(down_weight, 0)
+    gate_sum = jnp.dot(normed, gate, preferred_element_type=jnp.float32)
+    up_sum = jnp.dot(normed, up, preferred_element_type=jnp.float32)
+    hidden = (jax.nn.silu(gate_sum) * up_sum).astype(jnp.bfloat16)
+    down_sum = jnp.dot(hidden, down, preferred_element_type=jnp.float32).astype(jnp.bfloat16)
+    down_sum = lax.psum_scatter(down_sum, "sp", scatter_dimension=0, tiled=True)
+    return lax.psum_scatter(down_sum, "tp", scatter_dimension=1, tiled=True)
 
 
 def local(
@@ -126,6 +180,13 @@
     rescaled_portion = (
         resid_part * lax.rsqrt(elementwise_power / model_width + epsilon)[:, None] * gain_part
     ).astype(jnp.bfloat16)
+    places = lax.axis_size("sp")
+    hidden_share = gate_weight.shape[1]
+    moved = 2 * tokens * places * model_width
+    if moved < 3 * model_width * hidden_share and hidden_share % places == 0:
+        down_sum = spread_units(rescaled_portion, gate_weight, up_weight, down_weight)
+        ffn_part = down_sum.astype(jnp.float32)
+        return (resid_part + ffn_part).astype(jnp.bfloat16)
     normed = lax.all_gather(rescaled_portion, "tp", axis=1, tiled=True)
     gate_sum = jnp.dot(
         normed,

time: 431 us -> 257 us (0.60)
  waiting for transfers between devices: 363 us -> 125 us
  starting transfers between devices: 0.2 us -> 41.9 us
  local copies, waits for them, and re-layouts: 0.2 us -> 32 us
  blocking collectives: 25.3 us -> 18.4 us
    all_gather x3 -> x1, waiting for transfers between devices: 303 us -> 0.01 us  [spread_units(): normed = lax.all_gather(normed_part, ('sp', 'tp'))]
    reduce_scatter x1 -> x2, waiting for transfers between devices: 20 us -> 67.9 us  [the longest x1 44.7 us: spread_units(): down_sum = lax.psum_scatter(down_sum, 'sp', scatter_dimension=0, tiled=True)]
    ppermute x0 -> x18, starting transfers between devices: none -> 41.7 us  [the longest x9 31.6 us: swap_units(): pieces.append((shift, lax.ppermute(block, 'sp', ring)))]
    dynamic_update_slice x0 -> x21, local copies, waits for them, and re-layouts: none -> 17.2 us  [put(): return lax.dynamic_update_slice_in_dim(whole, block, at, other)]
    ppermute x0 -> x18, waiting for transfers between devices: none -> 16.9 us  [the longest x9 9.52 us: swap_units(): passed = lax.ppermute(block, 'grp', ring)]
    all_gather x1 -> x0, blocking collectives: 6.87 us -> none  [local(): normed = lax.all_gather(rescaled_portion, 'tp', axis=1, tiled=True)]
    dynamic_slice x0 -> x3, local copies, waits for them, and re-layouts: none -> 5.79 us  [swap_units(): block = lax.dynamic_slice_in_dim(block, copy * part, part, other)]
  transfers between devices with their start and end apart: 6 -> 23, of which waited for: 6 -> 10; matrix products, arithmetic and copies ran while one was open for 2% -> 11% of each run, Pallas kernels for 0% -> 0%
where the time goes in v1:
time: 257 us; the launch traced here: 256 us
  waiting for transfers between devices  125 us (49%)
  starting transfers between devices  41.9 us (16%)
  local copies, waits for them, and re-layouts  32 us (12%)
  blocking collectives  18.4 us (7%)
  matrix products  15.8 us (6%)
  between operations  13.5 us (5%)
  other arithmetic  10 us (4%)
    reduce_scatter x1, waiting for transfers between devices, spread_units(): down_sum = lax.psum_scatter(down_sum, 'sp', scatter_dimension=0, tiled=True)  44.7 us
    ppermute x9, starting transfers between devices, swap_units(): pieces.append((shift, lax.ppermute(block, 'sp', ring)))  31.6 us
    reduce_scatter x1, waiting for transfers between devices, spread_units(): return lax.psum_scatter(down_sum, 'tp', scatter_dimension=1, tiled=True)  23.2 us
    reduce_scatter x1, waiting for transfers between devices, local(): lax.psum_scatter(partial_out.astype(jnp.bfloat16), 'tp', scatter_dimensio...  23 us
    dynamic_update_slice x21, local copies, waits for them, and re-layouts, put(): return lax.dynamic_update_slice_in_dim(whole, block, at, other)  17.2 us
    all_gather x1, waiting for transfers between devices, carried_in(): lax.all_gather(a.astype(kind), axis)  16.6 us
    all_gather x1, blocking collectives, carried_in(): lax.all_gather(a.astype(kind), axis)  12.7 us
    ppermute x9, starting transfers between devices, swap_units(): passed = lax.ppermute(block, 'grp', ring)  10.1 us
  transfers between devices with their start and end apart: 23, of which 10 were waited for; matrix products, arithmetic and copies ran while one was open for 11% of the time, Pallas kernels for 0%

profile of v1, /device:TPU:0, one launch (start us, length us, event | category | flops | bytes accessed | tf_op | source)
XLA Modules:
  0.0 256.3 jit_solution(15068207768079115403)
XLA Ops:
  10.5 3.6 %while.26 = (s32[]{:T(128)}, f32[1,256,512]{2,1,0:T(8,128)S(1)}, f32[2,1,64,512]{3,2,1,0:T(8,128)}, f32[2,1,256]{2,1,0:T(1,128)S(1)}, f32[2,1,64,256]{3,2,1,0:T(...) while((s32[]{:T(128)}, f32[1,256,512]{2,1,0:T(8,128)S(1)}, ...), condition=%wide.region_2.3_spmd.clone, body=%wide.region_1.2_spmd.clone.sunk | while | flops 201850880 | bytes 1971308 | solution.py:148
  15.0 12.7 %all-gather.3 = bf16[4,1,256]{2,1,0:T(2,128)(2,1)S(1)} all-gather(bf16[1,1,256]{2,1,0:T(2,128)(2,1)S(1)} %reshape.253), channel_id=2, replica_groups=mesh['grp'=2,'sp'=4,'tp'=4] {'sp'}, dimensions={0}, use_global_device_ids=true | all-gather | bytes 2560 | tf_op jit(solution)/shard_map/all_gather | solution.py:19
  29.2 16.6 %all-gather.7.cloned.1.call-done = bf16[4,256,512]{2,1,0:T(8,128)(2,1)} async-done(((bf16[1,256,512]{2,1,0:T(8,128)(2,1)}), bf16[4,256,512]{2,1,0:T(8,128)(2,1)}) %all-gather.7.cloned.1.call-update) | async-done | bytes 1048592 | tf_op jit(solution)/shard_map/all_gather | solution.py:19
  49.6 23.0 %reduce-scatter.4.cloned.1.call-done = bf16[128,512]{1,0:T(8,128)(2,1)} async-done(((bf16[128,2048]{1,0:T(8,128)(2,1)}), bf16[128,512]{1,0:T(8,128)(2,1)}) %reduce-scatter.4.cloned.1.call-update) | async-done | bytes 131088 | tf_op jit(solution)/shard_map/reduce_scatter | solution.py:169
  73.8 5.8 %psum.7 = f32[128]{0:T(128)S(1)} all-reduce(f32[128]{0:T(128)S(1)} %multiply_reduce_fusion), channel_id=1, replica_groups=mesh['grp'=2,'sp'=4,'tp'=4] {'tp'}, use_global_device_ids=true, to_apply=%region_10.11 | all-reduce | flops 128 | bytes 1024 | tf_op jit(solution)/shard_map/psum | solution.py:176
  79.5 1.7 multiply_convert_fusion.2
  84.2 2.4 collective-permute-start.2
  88.1 2.3 fusion.38
  90.9 2.3 fusion.39
  97.1 2.0 dynamic-slice_dynamic-update-slice_fusion
  100.4 3.8 %collective-permute-start.8 = (bf16[256,352]{1,0:T(8,128)(2,1)}, bf16[256,352]{1,0:T(8,128)(2,1)S(1)}, u32[]{:S(2)}, u32[]{:S(2)}) collective-permute-start(bf16[256,352]{1,0:T(8,128)(2,1)} %get-tuple-element.179), channel_id=1, source_target_pairs={{0,8},{4,12},{8,0},{12,4},{1,9},{5,13},{9,1},{13,5},{2,10},{6,14},... | collective-permute-start | bytes 540680 | tf_op jit(solution)/shard_map/ppermute | solution.py:68
  105.8 7.4 %collective-permute-done.12 = bf16[352,256]{1,0:T(8,128)(2,1)} collective-permute-done((bf16[352,256]{1,0:T(8,128)(2,1)}, bf16[352,256]{1,0:T(8,128)(2,1)}, u32[]{:S(2)}, u32[]{:S(2)}) %collective-permute-start.12) | collective-permute-done | bytes 180256 | tf_op jit(solution)/shard_map/ppermute | solution.py:68
  118.2 1.7 collective-permute-done.1
  119.9 2.4 collective-permute-start.3
  125.4 19.5 %collective-permute-start.14 = (bf16[352,256]{1,0:T(8,128)(2,1)S(1)}, bf16[352,256]{1,0:T(8,128)(2,1)S(1)}, u32[]{:S(2)}, u32[]{:S(2)}) collective-permute-start(bf16[352,256]{1,0:T(8,128)(2,1)S(1)} %copy-done.7), channel_id=1, source_target_pairs={{0,8},{4,12},{8,0},{12,4},{1,9},{5,13},{9,1},{13,5},{2,10},{6,14},... | collective-permute-start | bytes 540680 | tf_op jit(solution)/shard_map/ppermute | solution.py:68
  145.7 1.7 collective-permute-start.16
  158.4 4.1 %collective-permute-done.15 = bf16[352,256]{1,0:T(8,128)(2,1)S(1)} collective-permute-done((bf16[352,256]{1,0:T(8,128)(2,1)S(1)}, bf16[352,256]{1,0:T(8,128)(2,1)S(1)}, u32[]{:S(2)}, u32[]{:S(2)}) %collective-permute-start.15) | collective-permute-done | bytes 180256 | tf_op jit(solution)/shard_map/ppermute | solution.py:75
  162.6 1.9 collective-permute-done.17
  165.9 3.2 %copy.24 = bf16[4,4,128,512]{3,1,2,0:T(4,128)(2,1)S(1)} copy(bf16[4,4,128,512]{3,2,1,0:T(8,128)(2,1)} %bitcast.124) | data formatting | bytes 4194304 | tf_op jit(solution)/shard_map/reshape | solution.py:85
  171.1 3.3 %fusion.42 = f32[512,352]{0,1:T(8,128)} fusion(bf16[512,2048]{1,0:T(8,128)(2,1)S(1)} %bitcast.125, bf16[2048,352]{1,0:T(8,128)(2,1)} %constant_dynamic-update-slice_fusion.11), kind=kOutput, calls=%fused_computation.99 | convolution fusion | flops 738197504 | bytes 4259840 | tf_op jit(solution)/shard_map/dot_general | solution.py:90
  174.4 5.7 %convolution_convert_fusion = bf16[512,2048]{1,0:T(8,128)(2,1)} fusion(bf16[352,2048]{1,0:T(8,128)(2,1)S(1)} %constant_dynamic-update-slice_fusion.10, f32[512,352]{0,1:T(8,128)} %fusion.42, bf16[512,2048]{1,0:T(8,128)(2,1)} %bitcast.126, bf16[2048,352]{1,0:T(8,128)(2,1)} %constant_dynamic-update-slice_fusion.4), kind=kOutput, calls=%fused_computation.20 | convolution fusion | flops 1478524928 | bytes 7798784 | tf_op jit(solution)/shard_map/dot_general | solution.py:93
  180.2 44.7 %reduce-scatter.6.cloned.1.call-done = bf16[128,2048]{1,0:T(8,128)(2,1)} async-done(((bf16[512,2048]{1,0:T(8,128)(2,1)}), bf16[128,2048]{1,0:T(8,128)(2,1)}) %reduce-scatter.6.cloned.1.call-update) | async-done | bytes 524304 | tf_op jit(solution)/shard_map/reduce_scatter | solution.py:94
  224.9 23.2 %reduce-scatter.8.cloned.1.call-done = bf16[128,512]{1,0:T(8,128)(2,1)} async-done(((bf16[128,2048]{1,0:T(8,128)(2,1)}), bf16[128,512]{1,0:T(8,128)(2,1)}) %reduce-scatter.8.cloned.1.call-update) | async-done | bytes 131088 | tf_op jit(solution)/shard_map/reduce_scatter | solution.py:95
  248.1 1.7 add_convert_fusion
  (120 shorter events, 49.7 us)
Async XLA Ops:
  6.5 39.3 %all-gather.7.cloned.1.call-start = ((), (), s32[]{:S(2)}) async-start(), calls=%async_computation.6 | async-start | bytes 1310720 | tf_op jit(solution)/shard_map/all_gather | solution.py:19
  14.9 57.7 %reduce-scatter.4.cloned.1.call-start = ((), (), s32[]{:S(2)}) async-start(), calls=%async_computation.3 | async-start | bytes 655360 | tf_op jit(solution)/shard_map/reduce_scatter | solution.py:169
  48.8 117.1 %all-gather.9.cloned.1.call-start = ((), (), s32[]{:S(2)}) async-start(), calls=%async_computation.7 | async-start | bytes 2228224 | tf_op jit(solution)/shard_map/all_gather | solution.py:81
  81.3 143.6 %reduce-scatter.6.cloned.1.call-start = ((), (), s32[]{:S(2)}) async-start(), calls=%async_computation.4 | async-start | bytes 2621440 | tf_op jit(solution)/shard_map/reduce_scatter | solution.py:94
  82.6 17.8 %collective-permute-start = (bf16[256,352]{1,0:T(8,128)(2,1)}, bf16[256,352]{1,0:T(8,128)(2,1)}, u32[]{:S(2)}, u32[]{:S(2)}) collective-permute-start(bf16[256,352]{1,0:T(8,128)(2,1)} %get-tuple-element.175), channel_id=1, source_target_pairs={{0,4},{4,8},{8,12},{12,0},{1,5},{5,9},{9,13},{13,1},{2,6},{6,10},{... | collective-permute-start | bytes 540680 | tf_op jit(solution)/shard_map/ppermute | solution.py:68
  84.2 33.4 %collective-permute-start.2 = (bf16[256,352]{1,0:T(8,128)(2,1)}, bf16[256,352]{1,0:T(8,128)(2,1)}, u32[]{:S(2)}, u32[]{:S(2)}) collective-permute-start(bf16[256,352]{1,0:T(8,128)(2,1)} %get-tuple-element.176), channel_id=1, source_target_pairs={{0,8},{4,12},{8,0},{12,4},{1,9},{5,13},{9,1},{13,5},{2,10},{6,14},... | collective-permute-start | bytes 540680 | tf_op jit(solution)/shard_map/ppermute | solution.py:68
  86.6 62.7 %collective-permute-start.4 = (bf16[256,352]{1,0:T(8,128)(2,1)}, bf16[256,352]{1,0:T(8,128)(2,1)}, u32[]{:S(2)}, u32[]{:S(2)}) collective-permute-start(bf16[256,352]{1,0:T(8,128)(2,1)} %get-tuple-element.174), channel_id=1, source_target_pairs={{0,12},{4,0},{8,4},{12,8},{1,13},{5,1},{9,5},{13,9},{2,14},{6,2},{... | collective-permute-start | bytes 540680 | tf_op jit(solution)/shard_map/ppermute | solution.py:68
  90.4 25.4 %collective-permute-start.6 = (bf16[256,352]{1,0:T(8,128)(2,1)}, bf16[256,352]{1,0:T(8,128)(2,1)}, u32[]{:S(2)}, u32[]{:S(2)}) collective-permute-start(bf16[256,352]{1,0:T(8,128)(2,1)} %get-tuple-element.178), channel_id=1, source_target_pairs={{0,4},{4,8},{8,12},{12,0},{1,5},{5,9},{9,13},{13,1},{2,6},{6,10},{... | collective-permute-start | bytes 540680 | tf_op jit(solution)/shard_map/ppermute | solution.py:68
  93.2 20.1 %collective-permute-start.12 = (bf16[352,256]{1,0:T(8,128)(2,1)}, bf16[352,256]{1,0:T(8,128)(2,1)}, u32[]{:S(2)}, u32[]{:S(2)}) collective-permute-start(bf16[352,256]{1,0:T(8,128)(2,1)} %get-tuple-element.181), channel_id=1, source_target_pairs={{0,4},{4,8},{8,12},{12,0},{1,5},{5,9},{9,13},{13,1},{2,6},{6,10},{... | collective-permute-start | bytes 540680 | tf_op jit(solution)/shard_map/ppermute | solution.py:68
  100.4 45.3 %collective-permute-start.8 = (bf16[256,352]{1,0:T(8,128)(2,1)}, bf16[256,352]{1,0:T(8,128)(2,1)S(1)}, u32[]{:S(2)}, u32[]{:S(2)}) collective-permute-start(bf16[256,352]{1,0:T(8,128)(2,1)} %get-tuple-element.179), channel_id=1, source_target_pairs={{0,8},{4,12},{8,0},{12,4},{1,9},{5,13},{9,1},{13,5},{2,10},{6,14},... | collective-permute-start | bytes 540680 | tf_op jit(solution)/shard_map/ppermute | solution.py:68
  113.2 6.6 %collective-permute-start.1 = (bf16[256,352]{1,0:T(8,128)(2,1)}, bf16[256,352]{1,0:T(8,128)(2,1)S(1)}, u32[]{:S(2)}, u32[]{:S(2)}) collective-permute-start(bf16[256,352]{1,0:T(8,128)(2,1)} %collective-permute-done), channel_id=1, source_target_pairs={{0,16},{16,0},{1,17},{17,1},{2,18},{18,2},{3,19},{19,3},{4,20},{20... | collective-permute-start | bytes 540680 | tf_op jit(solution)/shard_map/ppermute | solution.py:75
  115.8 35.0 %collective-permute-start.10 = (bf16[256,352]{1,0:T(8,128)(2,1)}, bf16[256,352]{1,0:T(8,128)(2,1)S(1)}, u32[]{:S(2)}, u32[]{:S(2)}) collective-permute-start(bf16[256,352]{1,0:T(8,128)(2,1)} %get-tuple-element.177), channel_id=1, source_target_pairs={{0,12},{4,0},{8,4},{12,8},{1,13},{5,1},{9,5},{13,9},{2,14},{6,2},{... | collective-permute-start | bytes 540680 | tf_op jit(solution)/shard_map/ppermute | solution.py:68
  117.6 7.8 %collective-permute-start.7 = (bf16[256,352]{1,0:T(8,128)(2,1)}, bf16[256,352]{1,0:T(8,128)(2,1)S(1)}, u32[]{:S(2)}, u32[]{:S(2)}) collective-permute-start(bf16[256,352]{1,0:T(8,128)(2,1)} %collective-permute-done.6), channel_id=1, source_target_pairs={{0,16},{16,0},{1,17},{17,1},{2,18},{18,2},{3,19},{19,3},{4,20},{20... | collective-permute-start | bytes 540680 | tf_op jit(solution)/shard_map/ppermute | solution.py:75
  119.9 27.5 %collective-permute-start.3 = (bf16[256,352]{1,0:T(8,128)(2,1)}, bf16[256,352]{1,0:T(8,128)(2,1)S(1)}, u32[]{:S(2)}, u32[]{:S(2)}) collective-permute-start(bf16[256,352]{1,0:T(8,128)(2,1)} %collective-permute-done.2), channel_id=1, source_target_pairs={{0,16},{16,0},{1,17},{17,1},{2,18},{18,2},{3,19},{19,3},{4,20},{20... | collective-permute-start | bytes 540680 | tf_op jit(solution)/shard_map/ppermute | solution.py:75
  125.4 25.9 %collective-permute-start.14 = (bf16[352,256]{1,0:T(8,128)(2,1)S(1)}, bf16[352,256]{1,0:T(8,128)(2,1)S(1)}, u32[]{:S(2)}, u32[]{:S(2)}) collective-permute-start(bf16[352,256]{1,0:T(8,128)(2,1)S(1)} %copy-done.7), channel_id=1, source_target_pairs={{0,8},{4,12},{8,0},{12,4},{1,9},{5,13},{9,1},{13,5},{2,10},{6,14},... | collective-permute-start | bytes 540680 | tf_op jit(solution)/shard_map/ppermute | solution.py:68
  145.7 7.1 %collective-permute-start.16 = (bf16[352,256]{1,0:T(8,128)(2,1)S(1)}, bf16[352,256]{1,0:T(8,128)(2,1)S(1)}, u32[]{:S(2)}, u32[]{:S(2)}) collective-permute-start(bf16[352,256]{1,0:T(8,128)(2,1)S(1)} %copy-done.6), channel_id=1, source_target_pairs={{0,12},{4,0},{8,4},{12,8},{1,13},{5,1},{9,5},{13,9},{2,14},{6,2},{... | collective-permute-start | bytes 540680 | tf_op jit(solution)/shard_map/ppermute | solution.py:68
  147.4 7.0 %collective-permute-start.13 = (bf16[352,256]{1,0:T(8,128)(2,1)}, bf16[352,256]{1,0:T(8,128)(2,1)S(1)}, u32[]{:S(2)}, u32[]{:S(2)}) collective-permute-start(bf16[352,256]{1,0:T(8,128)(2,1)} %collective-permute-done.12), channel_id=1, source_target_pairs={{0,16},{16,0},{1,17},{17,1},{2,18},{18,2},{3,19},{19,3},{4,20},{20... | collective-permute-start | bytes 540680 | tf_op jit(solution)/shard_map/ppermute | solution.py:75
  149.3 7.7 %collective-permute-start.9 = (bf16[256,352]{1,0:T(8,128)(2,1)S(1)}, bf16[256,352]{1,0:T(8,128)(2,1)S(1)}, u32[]{:S(2)}, u32[]{:S(2)}) collective-permute-start(bf16[256,352]{1,0:T(8,128)(2,1)S(1)} %collective-permute-done.8), channel_id=1, source_target_pairs={{0,16},{16,0},{1,17},{17,1},{2,18},{18,2},{3,19},{19,3},{4,20},{20... | collective-permute-start | bytes 540680 | tf_op jit(solution)/shard_map/ppermute | solution.py:75
  150.8 13.7 %collective-permute-start.5 = (bf16[256,352]{1,0:T(8,128)(2,1)}, bf16[256,352]{1,0:T(8,128)(2,1)S(1)}, u32[]{:S(2)}, u32[]{:S(2)}) collective-permute-start(bf16[256,352]{1,0:T(8,128)(2,1)} %collective-permute-done.4), channel_id=1, source_target_pairs={{0,16},{16,0},{1,17},{17,1},{2,18},{18,2},{3,19},{19,3},{4,20},{20... | collective-permute-start | bytes 540680 | tf_op jit(solution)/shard_map/ppermute | solution.py:75
  151.3 13.9 %collective-permute-start.11 = (bf16[256,352]{1,0:T(8,128)(2,1)S(1)}, bf16[256,352]{1,0:T(8,128)(2,1)S(1)}, u32[]{:S(2)}, u32[]{:S(2)}) collective-permute-start(bf16[256,352]{1,0:T(8,128)(2,1)S(1)} %collective-permute-done.10), channel_id=1, source_target_pairs={{0,16},{16,0},{1,17},{17,1},{2,18},{18,2},{3,19},{19,3},{4,20},{20... | collective-permute-start | bytes 540680 | tf_op jit(solution)/shard_map/ppermute | solution.py:75
  152.8 9.7 %collective-permute-start.15 = (bf16[352,256]{1,0:T(8,128)(2,1)S(1)}, bf16[352,256]{1,0:T(8,128)(2,1)S(1)}, u32[]{:S(2)}, u32[]{:S(2)}) collective-permute-start(bf16[352,256]{1,0:T(8,128)(2,1)S(1)} %collective-permute-done.14), channel_id=1, source_target_pairs={{0,16},{16,0},{1,17},{17,1},{2,18},{18,2},{3,19},{19,3},{4,20},{20... | collective-permute-start | bytes 540680 | tf_op jit(solution)/shard_map/ppermute | solution.py:75
  154.3 10.2 %collective-permute-start.17 = (bf16[352,256]{1,0:T(8,128)(2,1)S(1)}, bf16[352,256]{1,0:T(8,128)(2,1)S(1)}, u32[]{:S(2)}, u32[]{:S(2)}) collective-permute-start(bf16[352,256]{1,0:T(8,128)(2,1)S(1)} %collective-permute-done.16), channel_id=1, source_target_pairs={{0,16},{16,0},{1,17},{17,1},{2,18},{18,2},{3,19},{19,3},{4,20},{20... | collective-permute-start | bytes 540680 | tf_op jit(solution)/shard_map/ppermute | solution.py:75
  180.1 68.0 %copy-start.2 = (bf16[128,512]{1,0:T(8,128)(2,1)S(1)}, bf16[128,512]{1,0:T(8,128)(2,1)}, u32[]{:S(2)}) copy-start(bf16[128,512]{1,0:T(8,128)(2,1)} %reduce-scatter.4.cloned.1.call-done) | copy-start | bytes 393220
  180.1 68.0 %reduce-scatter.8.cloned.1.call-start = ((), (), s32[]{:S(2)}) async-start(), calls=%async_computation.5 | async-start | bytes 655360 | tf_op jit(solution)/shard_map/reduce_scatter | solution.py:95
  (10 other events, 169.7 us)
Sparse Core Ops, SparseCore 0:
  15.1 30.6 all-gather.6
  48.9 23.6 reduce-scatter.3
  81.4 55.1 all-gather.8
  180.3 44.6 reduce-scatter.5
  227.2 20.8 reduce-scatter.7

commit v2 on v0

--- a/solution.py
+++ b/solution.py
@@ -1,7 +1,10 @@
+import functools
 import jax
 import jax.numpy as jnp
 from jax import lax
 from jax.sharding import PartitionSpec as P
+from jax.experimental import pallas as pl
+from jax.experimental.pallas import tpu as pltpu
 
 HK = 256
 HV = 512
@@ -39,6 +42,438 @@
 
 def combine(earlier, later):
     return (earlier[0] * later[0], later[0][:, :, None] * earlier[1] + later[1])
+
+
+def nt_dot(a, b):
+    return lax.dot_general(a, b, (((1,), (1,)), ((), ())), preferred_element_type=jnp.float32)
+
+
+def fused_kernel(
+    places, shares, copies, units,
+    stream, queries, keys, values, out_gate, raw_score, extra_rate, head_gain, ffn_gain,
+    out_weight, gate_weight, up_weight, down_weight,
+    out,
+    gate_buf, up_buf, down_buf, wo_buf, state_own, state_in, decay_own, decay_in, attn,
+    proj_out, proj_in, resid, y_all, square_own, square_in, total,
+    pair_out, pair_in, held, cross_out, cross_in, line_out, line_in,
+    local_sem, wide_send, wide_recv, pass_send, pass_recv, state_send, state_recv,
+    decay_send, decay_recv, proj_send, proj_recv, square_send, square_recv,
+    total_send, total_recv, line_y_send, line_y_recv, core_send, core_recv,
+    chip_send, chip_recv, relay_send, relay_recv, pair_send, pair_recv,
+    cross_send, cross_recv, sum_send, sum_recv,
+):
+    s = lax.axis_index("sp")
+    t = lax.axis_index("tp")
+    g = lax.axis_index("grp")
+    f32, bf16 = jnp.float32, jnp.bfloat16
+    tokens = queries.shape[0]
+    cols = out.shape[1]
+    model_width = stream.shape[1]
+    depth = gate_weight.shape[0]
+    part = depth // copies
+    excess = places * units - gate_weight.shape[1]
+    blocks = tokens // BLOCK
+
+    def send(src, dst, send_sem, recv_sem, **where):
+        return pltpu.make_async_remote_copy(
+            src_ref=src, dst_ref=dst, send_sem=send_sem, recv_sem=recv_sem,
+            device_id=where, device_id_type=pl.DeviceIdType.MESH,
+        )
+
+    def up_by(k):
+        return lax.rem(s + k, places)
+
+    def down_by(k):
+        return lax.rem(s + places - k, places)
+
+    def offset(i):
+        return pl.multiple_of(i * units - (i // (places - 1)) * excess, 128)
+
+    weights = ((gate_weight, gate_buf), (up_weight, up_buf), (down_weight, down_buf))
+
+    def region(m, source, copy, size):
+        at = pl.ds(pl.multiple_of(source * depth + copy * part, 128), size)
+        return weights[m][1].at[:, at] if m == 2 else weights[m][1].at[at, :]
+
+    def source_of(m, target, copy, size):
+        at = pl.ds(pl.multiple_of(copy * part, 128), size)
+        chosen = pl.ds(offset(target), units)
+        return weights[m][0].at[chosen, at] if m == 2 else weights[m][0].at[at, chosen]
+
+    def wide(k, m):
+        return send(
+            source_of(m, up_by(k), g, part), region(m, s, g, part),
+            wide_send.at[k - 1, m], wide_recv.at[k - 1, m], sp=up_by(k),
+        )
+
+    def passed(k, m, turn):
+        here = region(m, down_by(k), g, part)
+        return send(
+            here, here, pass_send.at[turn - 1, k - 1, m], pass_recv.at[turn - 1, k - 1, m],
+            grp=lax.rem(g + turn, copies),
+        )
+
+    own = [
+        pltpu.make_async_copy(source_of(m, s, 0, depth), region(m, s, 0, depth), local_sem.at[m])
+        for m in range(3)
+    ]
+    load_out = pltpu.make_async_copy(out_weight, wo_buf, local_sem.at[3])
+    load_out.start()
+    for copy in own:
+        copy.start()
+
+    barrier = pltpu.get_barrier_semaphore()
+    for k in range(1, places):
+        pl.semaphore_signal(barrier, inc=1, device_id={"sp": up_by(k)}, device_id_type=pl.DeviceIdType.MESH)
+    for j in range(1, shares):
+        pl.semaphore_signal(
+            barrier, inc=1, device_id={"tp": lax.rem(t + j, shares)}, device_id_type=pl.DeviceIdType.MESH
+        )
+    for j in range(1, copies):
+        pl.semaphore_signal(
+            barrier, inc=1, device_id={"grp": lax.rem(g + j, copies)}, device_id_type=pl.DeviceIdType.MESH
+        )
+    pl.semaphore_wait(barrier, places + shares + copies - 3)
+
+    wide(1, 0).start()
+
+    score = raw_score[...]
+    decay = (
+        -(jnp.maximum(-score, 0.0) + jnp.log1p(jnp.exp(-jnp.abs(score)))) / sigmoid_sharpness
+        + extra_rate[...]
+    )
+    row = lax.broadcasted_iota(jnp.int32, (tokens, tokens), 0)
+    col = lax.broadcasted_iota(jnp.int32, (tokens, tokens), 1)
+    causal = row >= col
+    running = jnp.dot(
+        jnp.where(causal, 1.0, 0.0), decay, precision=highest, preferred_element_type=f32
+    )
+    last = running[tokens - 1 : tokens, :]
+    key = keys[...].astype(f32)
+    value = values[...]
+    key_end = (key * jnp.exp(last - running)).astype(bf16)
+    state_own[...] = lax.dot_general(
+        key_end, value, (((0,), (0,)), ((), ())), preferred_element_type=f32
+    ).astype(bf16)
+    decay_own[...] = jnp.broadcast_to(last, decay_own.shape)
+
+    def state_copies(k):
+        return (
+            send(decay_own, decay_in.at[k - 1], decay_send.at[k - 1], decay_recv.at[k - 1], sp=up_by(k)),
+            send(state_own, state_in.at[k - 1], state_send.at[k - 1], state_recv.at[k - 1], sp=up_by(k)),
+        )
+
+    for k in range(1, places):
+
+        @pl.when(s + k < places)
+        def _():
+            for copy in state_copies(k):
+                copy.start()
+
+    for k in range(2, places):
+        wide(k, 0).start()
+    for k in range(1, places):
+        wide(k, 1).start()
+
+    query = queries[...].astype(f32) * HK ** (-0.5)
+    pieces = []
+    for b in range(blocks):
+        rows = slice(b * BLOCK, (b + 1) * BLOCK)
+        begin = jnp.zeros_like(last) if b == 0 else running[b * BLOCK - 1 : b * BLOCK, :]
+        inner = running[rows] - begin
+        scores = nt_dot(
+            (query[rows] * jnp.exp(inner)).astype(bf16), (key[rows] * jnp.exp(-inner)).astype(bf16)
+        )
+        scores = jnp.where(causal[:BLOCK, :BLOCK], scores, 0.0).astype(bf16)
+        piece = jnp.dot(scores, value[rows], preferred_element_type=f32)
+        for c in range(b):
+            old = slice(c * BLOCK, (c + 1) * BLOCK)
+            close = running[(c + 1) * BLOCK - 1 : (c + 1) * BLOCK, :]
+            far = nt_dot(
+                (query[rows] * jnp.exp(running[rows] - close)).astype(bf16),
+                (key[old] * jnp.exp(close - running[old])).astype(bf16),
+            )
+            piece = piece + jnp.dot(far.astype(bf16), value[old], preferred_element_type=f32)
+        attn[rows, :] = piece
+
+    logits = out_gate[...].astype(f32)
+    gate_factor = head_gain[...] * (logits / (1.0 + jnp.exp(-logits)))
+    query_far = query * jnp.exp(running)
+    for k in range(1, places):
+
+        @pl.when(s >= k)
+        def _():
+            for copy in state_copies(k):
+                copy.wait_recv()
+            between = jnp.zeros_like(last)
+            for j in range(1, k):
+                between = between + decay_in[j - 1, 0:1, :]
+            attn[...] += jnp.dot(
+                (query_far * jnp.exp(between)).astype(bf16), state_in[k - 1],
+                preferred_element_type=f32,
+            )
+
+    heads = attn[...]
+    heads = heads * lax.rsqrt(jnp.mean(heads * heads, axis=-1, keepdims=True) + epsilon)
+    gated = (heads * gate_factor).astype(bf16)
+    load_out.wait()
+
+    def columns(i):
+        return pl.ds(pl.multiple_of(i * cols, 128), cols)
+
+    def proj_copy(j):
+        target = lax.rem(t + j, shares)
+        return send(
+            proj_out.at[j], proj_in.at[j - 1], proj_send.at[j - 1], proj_recv.at[j - 1], tp=target
+        )
+
+    for j in (2, 3, 1, 0) if shares == 4 else range(shares - 1, -1, -1):
+        target = lax.rem(t + j, shares)
+        proj_out[j] = jnp.dot(gated, wo_buf[:, columns(target)], preferred_element_type=f32).astype(bf16)
+        if j > 0:
+            proj_copy(j).start()
+
+    for k in range(1, places):
+        wide(k, 0).wait_recv()
+        for turn in range(1, copies):
+            passed(k, 0, turn).start()
+
+    joined = proj_out[0].astype(f32)
+    for j in range(1, shares):
+        proj_copy(j).wait_recv()
+        joined = joined + proj_in[j - 1].astype(f32)
+    joined = stream[:, columns(t)].astype(f32) + joined
+    resid[...] = joined
+    square_own[...] = lax.dot_general(
+        jnp.ones((8, cols), f32), joined * joined, (((1,), (1,)), ((), ())),
+        precision=highest, preferred_element_type=f32,
+    )
+    y_all[s, t] = (joined * ffn_gain[:, columns(t)].astype(f32)).astype(bf16)
+
+    def square_copy(j):
+        return send(
+            square_own, square_in.at[j - 1], square_send.at[j - 1], square_recv.at[j - 1],
+            tp=lax.rem(t + j, shares),
+        )
+
+    def total_copy(k):
+        return send(total.at[0], total.at[k], total_send.at[k - 1], total_recv.at[k - 1], sp=up_by(k))
+
+    def line_y(k):
+        mine = y_all.at[s, t]
+        return send(mine, mine, line_y_send.at[k - 1], line_y_recv.at[k - 1], sp=up_by(k))
+
+    half = shares // 2
+    near = t + 1 - 2 * lax.rem(t, 2)
+    across = lax.rem(t + half, shares)
+    diagonal = lax.rem(near + half, shares)
+
+    def core_y(k):
+        held_y = y_all.at[down_by(k), t]
+        return send(held_y, held_y, core_send.at[k], core_recv.at[k], tp=near)
+
+    def chip_y(k):
+        held_y = y_all.at[down_by(k), t]
+        return send(held_y, held_y, chip_send.at[k], chip_recv.at[k], tp=across)
+
+    def relay_y(k):
+        held_y = y_all.at[down_by(k), across]
+        return send(held_y, held_y, relay_send.at[k], relay_recv.at[k], tp=near)
+
+    for j in range(1, shares):
+        square_copy(j).start()
+    for k in range(1, places):
+        line_y(k).start()
+    chip_y(0).start()
+    core_y(0).start()
+    for k in range(1, places):
+        wide(k, 2).start()
+    squares = square_own[...]
+    for j in range(1, shares):
+        square_copy(j).wait_recv()
+        squares = squares + square_in[j - 1]
+    total[0] = squares
+    for k in range(1, places):
+        total_copy(k).start()
+    for k in range(1, places):
+        wide(k, 1).wait_recv()
+        for turn in range(1, copies):
+            passed(k, 1, turn).start()
+    chip_y(0).wait_recv()
+    relay_y(0).start()
+    for k in range(1, places):
+        line_y(k).wait_recv()
+        chip_y(k).start()
+        core_y(k).start()
+    for k in range(1, places):
+        chip_y(k).wait_recv()
+        relay_y(k).start()
+    for m in range(2):
+        own[m].wait()
+        for k in range(1, places):
+            for turn in range(1, copies):
+                passed(k, m, turn).wait_recv()
+    own[2].wait()
+    unit_at = lax.broadcasted_iota(jnp.int32, (tokens, units), 1)
+    keep = unit_at >= (s // (places - 1)) * excess
+    identity = jnp.where(row == col, 1.0, 0.0)
+
+    def pair_copy(k):
+        return send(pair_out.at[k], pair_in.at[k], pair_send.at[k], pair_recv.at[k], tp=near)
+
+    def cross_copy(k):
+        return send(cross_out.at[k], cross_in.at[k], cross_send.at[k], cross_recv.at[k], tp=across)
+
+    def sum_copy(k):
+        return send(line_out.at[k], line_in.at[k], sum_send.at[k], sum_recv.at[k], sp=down_by(k))
+
+    def pair_step(k):
+        pair_copy(k).wait_recv()
+        cross_out[k] = (held[k, 1] + pair_in[k, 1].astype(f32)).astype(bf16)
+        cross_copy(k).start()
+        held[k, 0] = held[k, 0] + pair_in[k, 0].astype(f32)
+
+    def cross_step(k):
+        cross_copy(k).wait_recv()
+        if k == 0:
+            held[k, 0] = held[k, 0] + cross_in[k].astype(f32)
+        else:
+            line_out[k] = (held[k, 0] + cross_in[k].astype(f32)).astype(bf16)
+            sum_copy(k).start()
+
+    order = list(range(1, places)) + [0]
+    for turn_at, k in enumerate(order):
+        block = down_by(k)
+        core_y(k).wait_recv()
+        relay_y(k).wait_recv()
+        if k > 0:
+            total_copy(k).wait_recv()
+        scale = lax.dot_general(
+            identity, total[k], (((1,), (1,)), ((), ())), precision=highest, preferred_element_type=f32
+        )[:, 0:1]
+        scale = lax.rsqrt(scale / model_width + epsilon)
+        gate_sum = jnp.zeros((tokens, units), f32)
+        up_sum = jnp.zeros((tokens, units), f32)
+        for i in range(shares):
+            y = y_all[block, i]
+            here = slice(i * cols, (i + 1) * cols)
+            gate_sum = gate_sum + jnp.dot(y, gate_buf[here, :], preferred_element_type=f32)
+            up_sum = up_sum + jnp.dot(y, up_buf[here, :], preferred_element_type=f32)
+        gate_sum = gate_sum * scale
+        up_sum = up_sum * scale
+        hidden = gate_sum / (1.0 + jnp.exp(-gate_sum)) * up_sum
+        hidden = jnp.where(keep, hidden, 0.0).astype(bf16)
+        if turn_at == 0:
+            for q in range(1, places):
+                wide(q, 2).wait_recv()
+                for turn in range(1, copies):
+                    passed(q, 2, turn).start()
+            for q in range(1, places):
+                for turn in range(1, copies):
+                    passed(q, 2, turn).wait_recv()
+        for i, target in enumerate((near, diagonal)):
+            pair_out[k, i] = jnp.dot(
+                hidden, down_buf[:, columns(target)], preferred_element_type=f32
+            ).astype(bf16)
+        pair_copy(k).start()
+        for i, target in enumerate((t, across)):
+            held[k, i] = jnp.dot(hidden, down_buf[:, columns(target)], preferred_element_type=f32)
+        if turn_at > 0:
+            pair_step(order[turn_at - 1])
+        if turn_at > 1:
+            cross_step(order[turn_at - 2])
+    pair_step(order[-1])
+    for k in order[-2:]:
+        cross_step(k)
+    result = resid[...] + held[0, 0]
+    for k in range(1, places):
+        sum_copy(k).wait_recv()
+        result = result + line_in[k].astype(f32)
+    out[...] = result.astype(bf16)
+
+    for k in range(1, places):
+
+        @pl.when(s + k < places)
+        def _():
+            for copy in state_copies(k):
+                copy.wait_send()
+
+        for m in range(3):
+            wide(k, m).wait_send()
+            for turn in range(1, copies):
+                passed(k, m, turn).wait_send()
+        total_copy(k).wait_send()
+        line_y(k).wait_send()
+        sum_copy(k).wait_send()
+    for j in range(1, shares):
+        proj_copy(j).wait_send()
+        square_copy(j).wait_send()
+    for k in range(places):
+        for copy in (core_y, chip_y, relay_y, pair_copy, cross_copy):
+            copy(k).wait_send()
+
+
+def fused(units, *arrays):
+    (
+        stream, queries, key_matrix, value_matrix, output_gate_logits, forgetting_raw_score,
+        additional_forgetting_rate, head_norm_gain, output_weight, feedforward_norm_gain,
+        gate_weight, up_weight, down_weight,
+    ) = arrays
+    places, shares, copies = (lax.axis_size(a) for a in ("sp", "tp", "grp"))
+    tokens, model_width = stream.shape
+    cols = model_width // shares
+    f32, bf16 = jnp.float32, jnp.bfloat16
+    vmem = pl.BlockSpec(memory_space=pltpu.VMEM)
+    anywhere = pl.BlockSpec(memory_space=pl.ANY)
+    buffers = [
+        ((model_width, units), bf16), ((model_width, units), bf16), ((units, model_width), bf16),
+        (output_weight.shape, bf16), ((HK, HV), bf16), ((places - 1, HK, HV), bf16),
+        ((8, HK), f32), ((places - 1, 8, HK), f32), ((tokens, HV), f32),
+        ((shares, tokens, cols), bf16), ((shares - 1, tokens, cols), bf16), ((tokens, cols), f32),
+        ((places, shares, tokens, cols), bf16), ((8, tokens), f32), ((shares - 1, 8, tokens), f32),
+        ((places, 8, tokens), f32),
+        ((places, 2, tokens, cols), bf16), ((places, 2, tokens, cols), bf16),
+        ((places, 2, tokens, cols), f32),
+        ((places, tokens, cols), bf16), ((places, tokens, cols), bf16),
+        ((places, tokens, cols), bf16), ((places, tokens, cols), bf16),
+    ]
+    far = places - 1
+    counts = [(4,)]
+    for count in (
+        (far, 3), (copies - 1, far, 3), (far,), (far,), (shares - 1,), (shares - 1,), (far,), (far,),
+        (places,), (places,), (places,), (places,), (places,), (places,),
+    ):
+        counts += [count, count]
+    kernel = functools.partial(fused_kernel, places, shares, copies, units)
+    return pl.pallas_call(
+        kernel,
+        out_shape=jax.ShapeDtypeStruct((tokens, cols), bf16),
+        in_specs=[vmem] * 9 + [anywhere] * 4,
+        out_specs=vmem,
+        scratch_shapes=[pltpu.VMEM(shape, kind) for shape, kind in buffers]
+        + [pltpu.SemaphoreType.DMA(count) for count in counts],
+        compiler_params=pltpu.CompilerParams(
+            collective_id=0, has_side_effects=True, vmem_limit_bytes=58 * 1024 * 1024
+        ),
+    )(
+        stream, queries, key_matrix, value_matrix, output_gate_logits, forgetting_raw_score,
+        additional_forgetting_rate, head_norm_gain.reshape(1, -1), feedforward_norm_gain.reshape(1, -1),
+        output_weight, gate_weight, up_weight, down_weight,
+    )
+
+
+def spread_width(stream, queries, gate_weight):
+    places, shares, copies = (lax.axis_size(a) for a in ("sp", "tp", "grp"))
+    tokens, model_width = stream.shape
+    depth, hidden_share = gate_weight.shape
+    units = -(-hidden_share // (places * 128)) * 128
+    fits = (
+        shares == 4 and places > 1 and copies > 1 and queries.shape[1] == HK
+        and tokens % 128 == 0 and model_width % (shares * 128) == 0 and depth % (copies * 128) == 0
+        and hidden_share % 128 == 0 and places * units - hidden_share < units
+        and 2 * tokens * places < 3 * hidden_share
+    )
+    return units if fits else 0
 
 
 def local(
@@ -56,6 +491,13 @@
     up_weight,
     down_weight,
 ):
+    units = spread_width(stream, queries, gate_weight)
+    if units:
+        return fused(
+            units, stream, queries, key_matrix, value_matrix, output_gate_logits,
+            forgetting_raw_score, additional_forgetting_rate, head_norm_gain, output_weight,
+            feedforward_norm_gain, gate_weight, up_weight, down_weight,
+        )
     tokens = queries.shape[0]
     owned_heads = queries.shape[1] // HK
     blocks = tokens // BLOCK

time: 431 us -> 132 us (0.31)
  waiting for transfers between devices: 363 us -> 0 us
  Pallas kernels: 0 us -> 129 us
  blocking collectives: 25.3 us -> 0 us
  matrix products: 17.6 us -> 0 us
  between operations: 13.7 us -> 0.01 us
  other arithmetic: 10.2 us -> 0 us
    all_gather x4 -> x0, waiting for transfers between devices: 319 us -> none  [the longest x1 106 us: local(): lax.all_gather(down_weight, 'sp', axis=1, tiled=True)]
    pallas_call x0 -> x1, Pallas kernels: none -> 129 us  [fused(): pl.pallas_call(kernel, out_shape=jax.ShapeDtypeStruct((tokens, cols), bf1...]
    reduce_scatter x2 -> x0, waiting for transfers between devices: 42.1 us -> none  [the longest x1 22.1 us: local(): lax.psum_scatter(partial_out.astype(jnp.bfloat16), 'tp', scatter_dimensio...]
    all_gather x2 -> x0, blocking collectives: 19.5 us -> none  [the longest x1 12.6 us: carried_in(): lax.all_gather(a.astype(kind), axis)]
    dot_general x10 -> x0, matrix products: 17.6 us -> none  [the longest x1 7.03 us: local(): jnp.dot(hidden, lax.all_gather(down_weight, 'sp', axis=1, tiled=True), pr...]
    psum x1 -> x0, blocking collectives: 5.76 us -> none  [local(): elementwise_power = lax.psum(jnp.sum(resid_part * resid_part, axis=1), 'tp')]
    convert_element_type x7 -> x0, other arithmetic: 5.21 us -> none  [the longest x1 1.67 us: local(): return (resid_part + ffn_part).astype(jnp.bfloat16)]
  transfers between devices with their start and end apart: 6 -> 0, of which waited for: 6 -> 0; matrix products, arithmetic and copies ran while one was open for 2% -> 0% of each run, Pallas kernels for 0% -> 0%
where the time goes in v2:
time: 132 us
  Pallas kernels  129 us (98%)
  local copies, waits for them, and re-layouts  2.86 us (2%)
    pallas_call x1, Pallas kernels, fused(): pl.pallas_call(kernel, out_shape=jax.ShapeDtypeStruct((tokens, cols), bf1...  129 us

profile of v2, /device:TPU:0, one launch (start us, length us, event | category | flops | bytes accessed | tf_op | source)
XLA Modules:
  0.0 132.3 jit_solution(5165548712030788200)
XLA Ops:
  0.0 1.3 reshape.7.ffn_gain
  1.3 129.4 %shard_map.127 = bf16[128,512]{1,0:T(8,128)(2,1)} custom-call(bf16[128,2048]{1,0:T(8,128)(2,1)} %stream.1, bf16[128,256]{1,0:T(8,128)(2,1)} %queries.1, bf16[128,256]{1,0:T(8,128)(2,1)} %keys.1, bf16[128,512]{1,0:T(8,128)(2,1)} %values.1, bf16[128,512]{1,0:T(8,128)(2,1)} %out_gate.1, f32[128,256]{1,0:T(8,128)} %raw_score.1, f32[128,256]{1,0:T(8,128)} %extra_rate.1, ...), custom_call_target="tpu_custom_call" | custom-call | tf_op jit(solution)/shard_map/pallas_call | solution.py:448
  130.7 1.6 %copy.15 = bf16[128,512]{1,0:T(8,128)(2,1)} copy(bf16[128,512]{1,0:T(8,128)(2,1)} %shard_map.127) | data formatting | bytes 262144

commit v3 on v2

--- a/solution.py
+++ b/solution.py
@@ -53,12 +53,12 @@
     stream, queries, keys, values, out_gate, raw_score, extra_rate, head_gain, ffn_gain,
     out_weight, gate_weight, up_weight, down_weight,
     out,
-    gate_buf, up_buf, down_buf, wo_buf, state_own, state_in, decay_own, decay_in, attn,
+    gate_buf, up_buf, down_buf, wo_buf, state_own, state_out, state_in, hidden_all, attn,
     proj_out, proj_in, resid, y_all, square_own, square_in, total,
     pair_out, pair_in, held, cross_out, cross_in, line_out, line_in,
     local_sem, wide_send, wide_recv, pass_send, pass_recv, state_send, state_recv,
-    decay_send, decay_recv, proj_send, proj_recv, square_send, square_recv,
-    total_send, total_recv, line_y_send, line_y_recv, core_send, core_recv,
+    proj_send, proj_recv, square_send, square_recv,
+    total_send, total_recv, up_send, up_recv, down_send, down_recv, core_send, core_recv,
     chip_send, chip_recv, relay_send, relay_recv, pair_send, pair_recv,
     cross_send, cross_recv, sum_send, sum_recv,
 ):
@@ -86,8 +86,7 @@
     def down_by(k):
         return lax.rem(s + places - k, places)
 
-    def offset(i):
-        return pl.multiple_of(i * units - (i // (places - 1)) * excess, 128)
+    short = units - excess
 
     weights = ((gate_weight, gate_buf), (up_weight, up_buf), (down_weight, down_buf))
 
@@ -95,32 +94,102 @@
         at = pl.ds(pl.multiple_of(source * depth + copy * part, 128), size)
         return weights[m][1].at[:, at] if m == 2 else weights[m][1].at[at, :]
 
-    def source_of(m, target, copy, size):
+    def taken(m, ref, size):
+        return ref.at[0:size, :] if m == 2 else ref.at[:, 0:size]
+
+    def source_of(m, target, copy, size, width):
         at = pl.ds(pl.multiple_of(copy * part, 128), size)
-        chosen = pl.ds(offset(target), units)
+        back = target // (places - 1) * excess if width == units else 0
+        chosen = pl.ds(pl.multiple_of(target * units - back, 128), width)
         return weights[m][0].at[chosen, at] if m == 2 else weights[m][0].at[at, chosen]
 
-    def wide(k, m):
+    def wide_copy(k, m, width):
         return send(
-            source_of(m, up_by(k), g, part), region(m, s, g, part),
+            source_of(m, up_by(k), g, part, width), taken(m, region(m, s, g, part), width),
             wide_send.at[k - 1, m], wide_recv.at[k - 1, m], sp=up_by(k),
         )
 
-    def passed(k, m, turn):
-        here = region(m, down_by(k), g, part)
+    def pass_copy(k, m, turn, width):
+        here = taken(m, region(m, down_by(k), g, part), width)
         return send(
             here, here, pass_send.at[turn - 1, k - 1, m], pass_recv.at[turn - 1, k - 1, m],
             grp=lax.rem(g + turn, copies),
         )
 
-    own = [
-        pltpu.make_async_copy(source_of(m, s, 0, depth), region(m, s, 0, depth), local_sem.at[m])
-        for m in range(3)
-    ]
+    def own_copy(m, width):
+        return pltpu.make_async_copy(
+            source_of(m, s, 0, depth, width), taken(m, region(m, s, 0, depth), width), local_sem.at[m]
+        )
+
+    def by_width(place, act):
+        if excess == 0:
+            act(units)
+            return
+
+        @pl.when(place == places - 1)
+        def _():
+            act(short)
+
+        @pl.when(place != places - 1)
+        def _():
+            act(units)
+
+    def wide_start(k, m):
+        by_width(up_by(k), lambda width: wide_copy(k, m, width).start())
+
+    def wide_sent(k, m):
+        by_width(up_by(k), lambda width: wide_copy(k, m, width).wait_send())
+
+    def arrive_and_pass(k, m):
+        def act(width):
+            wide_copy(k, m, width).wait_recv()
+            for turn in range(1, copies):
+                pass_copy(k, m, turn, width).start()
+
+        by_width(s, act)
+
+    def pass_arrive(m):
+        def act(width):
+            own_copy(m, width).wait()
+            for k in range(1, places):
+                for turn in range(1, copies):
+                    pass_copy(k, m, turn, width).wait_recv()
+
+        by_width(s, act)
+
+    def pass_sent(m):
+        def act(width):
+            for k in range(1, places):
+                for turn in range(1, copies):
+                    pass_copy(k, m, turn, width).wait_send()
+
+        by_width(s, act)
+
+    def start_upward(k, m):
+        @pl.when(s + k < places)
+        def _():
+            wide_start(k, m)
+
+    def start_downward(k, m):
+        @pl.when(s + k >= places)
+        def _():
+            wide_start(k, m)
+
     load_out = pltpu.make_async_copy(out_weight, wo_buf, local_sem.at[3])
     load_out.start()
-    for copy in own:
-        copy.start()
+
+    def own_start(width):
+        for m in range(3):
+            own_copy(m, width).start()
+
+    by_width(s, own_start)
+    if excess > 0:
+
+        @pl.when(s == places - 1)
+        def _():
+            gate_buf[:, short:] = jnp.zeros((model_width, excess), bf16)
+            up_buf[:, short:] = jnp.zeros((model_width, excess), bf16)
+            down_buf[short:, :] = jnp.zeros((excess, model_width), bf16)
 
     barrier = pltpu.get_barrier_semaphore()
     for k in range(1, places):
@@ -135,7 +204,11 @@
         )
     pl.semaphore_wait(barrier, places + shares + copies - 3)
 
-    wide(1, 0).start()
+    far_first = list(range(places // 2, places)) + list(range(1, places // 2))
+    start_upward(far_first[0], 0)
+    for m in range(2):
+        for k in range(places - 1, 0, -1):
+            start_downward(k, m)
 
     score = raw_score[...]
     decay = (
@@ -154,26 +227,26 @@
     key_end = (key * jnp.exp(last - running)).astype(bf16)
     state_own[...] = lax.dot_general(
         key_end, value, (((0,), (0,)), ((), ())), preferred_element_type=f32
-    ).astype(bf16)
-    decay_own[...] = jnp.broadcast_to(last, decay_own.shape)
-
-    def state_copies(k):
-        return (
-            send(decay_own, decay_in.at[k - 1], decay_send.at[k - 1], decay_recv.at[k - 1], sp=up_by(k)),
-            send(state_own, state_in.at[k - 1], state_send.at[k - 1], state_recv.at[k - 1], sp=up_by(k)),
-        )
-
-    for k in range(1, places):
-
-        @pl.when(s + k < places)
-        def _():
-            for copy in state_copies(k):
-                copy.start()
-
-    for k in range(2, places):
-        wide(k, 0).start()
-    for k in range(1, places):
-        wide(k, 1).start()
+    )
+    kept = jnp.exp(
+        lax.dot_general(
+            decay, jnp.ones((tokens, 128), f32), (((0,), (0,)), ((), ())),
+            precision=highest, preferred_element_type=f32,
+        )
+    )
+    chunks = state_out.shape[0]
+
+    def state_copy(c):
+        return send(
+            state_out.at[c], state_in.at[c], state_send.at[c], state_recv.at[c],
+            sp=lax.rem(s + 1, places),
+        )
+
+    @pl.when(s == 0)
+    def _():
+        for c in range(chunks):
+            state_out[c] = state_own[:, c * 128 : (c + 1) * 128].astype(bf16)
+            state_copy(c).start()
 
     query = queries[...].astype(f32) * HK ** (-0.5)
     pieces = []
@@ -199,19 +272,27 @@
     logits = out_gate[...].astype(f32)
     gate_factor = head_gain[...] * (logits / (1.0 + jnp.exp(-logits)))
     query_far = query * jnp.exp(running)
-    for k in range(1, places):
-
-        @pl.when(s >= k)
-        def _():
-            for copy in state_copies(k):
-                copy.wait_recv()
-            between = jnp.zeros_like(last)
-            for j in range(1, k):
-                between = between + decay_in[j - 1, 0:1, :]
-            attn[...] += jnp.dot(
-                (query_far * jnp.exp(between)).astype(bf16), state_in[k - 1],
-                preferred_element_type=f32,
-            )
+    far_query = query_far.astype(bf16)
+
+    @pl.when(s > 0)
+    def _():
+        for c in range(chunks):
+            here = slice(c * 128, (c + 1) * 128)
+            state_copy(c).wait_recv()
+
+            @pl.when(s < places - 1)
+            def _():
+                state_out[c] = (kept * state_in[c].astype(f32) + state_own[:, here]).astype(bf16)
+                state_copy(c).start()
+
+        for c in range(chunks):
+            here = slice(c * 128, (c + 1) * 128)
+            attn[:, here] += jnp.dot(far_query, state_in[c], preferred_element_type=f32)
+
+    for k in far_first[1:]:
+        start_upward(k, 0)
+    for k in far_first:
+        start_upward(k, 1)
 
     heads = attn[...]
     heads = heads * lax.rsqrt(jnp.mean(heads * heads, axis=-1, keepdims=True) + epsilon)
@@ -232,11 +313,6 @@
         proj_out[j] = jnp.dot(gated, wo_buf[:, columns(target)], preferred_element_type=f32).astype(bf16)
         if j > 0:
             proj_copy(j).start()
-
-    for k in range(1, places):
-        wide(k, 0).wait_recv()
-        for turn in range(1, copies):
-            passed(k, 0, turn).start()
 
     joined = proj_out[0].astype(f32)
     for j in range(1, shares):
@@ -259,9 +335,31 @@
     def total_copy(k):
         return send(total.at[0], total.at[k], total_send.at[k - 1], total_recv.at[k - 1], sp=up_by(k))
 
-    def line_y(k):
-        mine = y_all.at[s, t]
-        return send(mine, mine, line_y_send.at[k - 1], line_y_recv.at[k - 1], sp=up_by(k))
+    def up_y(k):
+        held_y = y_all.at[down_by(k - 1), t]
+        return send(held_y, held_y, up_send.at[k - 1], up_recv.at[k - 1], sp=lax.rem(s + 1, places))
+
+    def down_y(k):
+        held_y = y_all.at[up_by(k - 1), t]
+        return send(
+            held_y, held_y, down_send.at[k - 1], down_recv.at[k - 1], sp=lax.rem(s + places - 1, places)
+        )
+
+    def pass_up(k, finish=False):
+        @pl.when(jnp.logical_and(s + 1 < places, s >= k - 1))
+        def _():
+            if finish:
+                up_y(k).wait_send()
+            else:
+                up_y(k).start()
+
+    def pass_down(k, finish=False):
+        @pl.when(jnp.logical_and(s >= 1, s + k - 1 < places))
+        def _():
+            if finish:
+                down_y(k).wait_send()
+            else:
+                down_y(k).start()
 
     half = shares // 2
     near = t + 1 - 2 * lax.rem(t, 2)
@@ -282,12 +380,14 @@
 
     for j in range(1, shares):
         square_copy(j).start()
-    for k in range(1, places):
-        line_y(k).start()
+    pass_up(1)
+    pass_down(1)
     chip_y(0).start()
     core_y(0).start()
     for k in range(1, places):
-        wide(k, 2).start()
+        wide_start(far_first[k - 1], 2)
+    for k in range(1, places):
+        arrive_and_pass(k, 0)
     squares = square_own[...]
     for j in range(1, shares):
         square_copy(j).wait_recv()
@@ -296,26 +396,34 @@
     for k in range(1, places):
         total_copy(k).start()
     for k in range(1, places):
-        wide(k, 1).wait_recv()
-        for turn in range(1, copies):
-            passed(k, 1, turn).start()
+        arrive_and_pass(k, 1)
     chip_y(0).wait_recv()
     relay_y(0).start()
     for k in range(1, places):
-        line_y(k).wait_recv()
-        chip_y(k).start()
-        core_y(k).start()
+
+        @pl.when(s >= k)
+        def _():
+            up_y(k).wait_recv()
+            if k + 1 < places:
+                pass_up(k + 1)
+            chip_y(k).start()
+            core_y(k).start()
+
+        @pl.when(s + k < places)
+        def _():
+            down_y(k).wait_recv()
+            if k + 1 < places:
+                pass_down(k + 1)
+            chip_y(places - k).start()
+            core_y(places - k).start()
+
     for k in range(1, places):
         chip_y(k).wait_recv()
         relay_y(k).start()
     for m in range(2):
-        own[m].wait()
-        for k in range(1, places):
-            for turn in range(1, copies):
-                passed(k, m, turn).wait_recv()
-    own[2].wait()
+        pass_arrive(m)
     unit_at = lax.broadcasted_iota(jnp.int32, (tokens, units), 1)
-    keep = unit_at >= (s // (places - 1)) * excess
+    keep = unit_at < units - (s // (places - 1)) * excess
     identity = jnp.where(row == col, 1.0, 0.0)
 
     def pair_copy(k):
@@ -342,7 +450,7 @@
             sum_copy(k).start()
 
     order = list(range(1, places)) + [0]
-    for turn_at, k in enumerate(order):
+    for turn_at, k in enumerate([0] + list(range(1, places))):
         block = down_by(k)
         core_y(k).wait_recv()
         relay_y(k).wait_recv()
@@ -362,15 +470,12 @@
         gate_sum = gate_sum * scale
         up_sum = up_sum * scale
         hidden = gate_sum / (1.0 + jnp.exp(-gate_sum)) * up_sum
-        hidden = jnp.where(keep, hidden, 0.0).astype(bf16)
-        if turn_at == 0:
-            for q in range(1, places):
-                wide(q, 2).wait_recv()
-                for turn in range(1, copies):
-                    passed(q, 2, turn).start()
-            for q in range(1, places):
-                for turn in range(1, copies):
-                    passed(q, 2, turn).wait_recv()
+        hidden_all[k] = jnp.where(keep, hidden, 0.0).astype(bf16)
+        if k > 0:
+            arrive_and_pass(k, 2)
+    pass_arrive(2)
+    for turn_at, k in enumerate(order):
+        hidden = hidden_all[k]
         for i, target in enumerate((near, diagonal)):
             pair_out[k, i] = jnp.dot(
                 hidden, down_buf[:, columns(target)], preferred_element_type=f32
@@ -391,20 +496,20 @@
         result = result + line_in[k].astype(f32)
     out[...] = result.astype(bf16)
 
-    for k in range(1, places):
-
-        @pl.when(s + k < places)
-        def _():
-            for copy in state_copies(k):
-                copy.wait_send()
-
+    @pl.when(s < places - 1)
+    def _():
+        for c in range(chunks):
+            state_copy(c).wait_send()
+
+    for k in range(1, places):
         for m in range(3):
-            wide(k, m).wait_send()
-            for turn in range(1, copies):
-                passed(k, m, turn).wait_send()
+            wide_sent(k, m)
+        pass_up(k, True)
+        pass_down(k, True)
         total_copy(k).wait_send()
-        line_y(k).wait_send()
         sum_copy(k).wait_send()
+    for m in range(3):
+        pass_sent(m)
     for j in range(1, shares):
         proj_copy(j).wait_send()
         square_copy(j).wait_send()
@@ -427,8 +532,8 @@
     anywhere = pl.BlockSpec(memory_space=pl.ANY)
     buffers = [
         ((model_width, units), bf16), ((model_width, units), bf16), ((units, model_width), bf16),
-        (output_weight.shape, bf16), ((HK, HV), bf16), ((places - 1, HK, HV), bf16),
-        ((8, HK), f32), ((places - 1, 8, HK), f32), ((tokens, HV), f32),
+        (output_weight.shape, bf16), ((HK, HV), f32), ((HV // 128, HK, 128), bf16),
+        ((HV // 128, HK, 128), bf16), ((places, tokens, units), bf16), ((tokens, HV), f32),
         ((shares, tokens, cols), bf16), ((shares - 1, tokens, cols), bf16), ((tokens, cols), f32),
         ((places, shares, tokens, cols), bf16), ((8, tokens), f32), ((shares - 1, 8, tokens), f32),
         ((places, 8, tokens), f32),
@@ -440,7 +545,7 @@
     far = places - 1
     counts = [(4,)]
     for count in (
-        (far, 3), (copies - 1, far, 3), (far,), (far,), (shares - 1,), (shares - 1,), (far,), (far,),
+        (far, 3), (copies - 1, far, 3), (HV // 128,), (shares - 1,), (shares - 1,), (far,), (far,), (far,),
         (places,), (places,), (places,), (places,), (places,), (places,),
     ):
         counts += [count, count]

time: 132 us -> 110 us (0.83)
  Pallas kernels: 129 us -> 107 us
    pallas_call x1, Pallas kernels: 129 us -> 107 us  [fused(): pl.pallas_call(kernel, out_shape=jax.ShapeDtypeStruct((tokens, cols), bf1...]
where the time goes in v3:
time: 110 us
  Pallas kernels  107 us (97%)
  local copies, waits for them, and re-layouts  2.86 us (3%)
    pallas_call x1, Pallas kernels, fused(): pl.pallas_call(kernel, out_shape=jax.ShapeDtypeStruct((tokens, cols), bf1...  107 us

profile of v3, /device:TPU:0, one launch (start us, length us, event | category | flops | bytes accessed | tf_op | source)
XLA Modules:
  0.0 109.7 jit_solution(8709860691585910447)
XLA Ops:
  0.0 1.3 %reshape.7.ffn_gain = bf16[1,2048]{1,0:T(2,128)(2,1)} reshape(bf16[2048]{0:T(1024)(128)(2,1)} %param.22) | data formatting | bytes 8192 | tf_op jit(solution)/shard_map/reshape | solution.py:565
  1.3 106.8 %shard_map.127 = bf16[128,512]{1,0:T(8,128)(2,1)} custom-call(bf16[128,2048]{1,0:T(8,128)(2,1)} %stream.1, bf16[128,256]{1,0:T(8,128)(2,1)} %queries.1, bf16[128,256]{1,0:T(8,128)(2,1)} %keys.1, bf16[128,512]{1,0:T(8,128)(2,1)} %values.1, bf16[128,512]{1,0:T(8,128)(2,1)} %out_gate.1, f32[128,256]{1,0:T(8,128)} %raw_score.1, f32[128,256]{1,0:T(8,128)} %extra_rate.1, ...), custom_call_target="tpu_custom_call" | custom-call | tf_op jit(solution)/shard_map/pallas_call | solution.py:553
  108.1 1.6 %copy.15 = bf16[128,512]{1,0:T(8,128)(2,1)} copy(bf16[128,512]{1,0:T(8,128)(2,1)} %shard_map.127) | data formatting | bytes 262144

commit v4 on v3

--- a/solution.py
+++ b/solution.py
@@ -58,7 +58,7 @@
     pair_out, pair_in, held, cross_out, cross_in, line_out, line_in,
     local_sem, wide_send, wide_recv, pass_send, pass_recv, state_send, state_recv,
     proj_send, proj_recv, square_send, square_recv,
-    total_send, total_recv, up_send, up_recv, down_send, down_recv, core_send, core_recv,
+    total_send, total_recv, line_y_send, line_y_recv, core_send, core_recv,
     chip_send, chip_recv, relay_send, relay_recv, pair_send, pair_recv,
     cross_send, cross_recv, sum_send, sum_recv,
 ):
@@ -248,6 +248,21 @@
             state_out[c] = state_own[:, c * 128 : (c + 1) * 128].astype(bf16)
             state_copy(c).start()
 
+    @pl.when(s > 0)
+    def _():
+        for c in range(chunks):
+            here = slice(c * 128, (c + 1) * 128)
+            state_copy(c).wait_recv()
+
+            @pl.when(s < places - 1)
+            def _():
+                state_out[c] = (kept * state_in[c].astype(f32) + state_own[:, here]).astype(bf16)
+                state_copy(c).start()
+
+    for k in far_first[1:]:
+        start_upward(k, 0)
+    for k in far_first:
+        start_upward(k, 1)
     query = queries[...].astype(f32) * HK ** (-0.5)
     pieces = []
     for b in range(blocks):
@@ -278,21 +293,13 @@
     def _():
         for c in range(chunks):
             here = slice(c * 128, (c + 1) * 128)
-            state_copy(c).wait_recv()
-
-            @pl.when(s < places - 1)
-            def _():
-                state_out[c] = (kept * state_in[c].astype(f32) + state_own[:, here]).astype(bf16)
-                state_copy(c).start()
-
-        for c in range(chunks):
-            here = slice(c * 128, (c + 1) * 128)
             attn[:, here] += jnp.dot(far_query, state_in[c], preferred_element_type=f32)
 
-    for k in far_first[1:]:
-        start_upward(k, 0)
-    for k in far_first:
-        start_upward(k, 1)
+    for k in range(places - 1, 0, -1):
+
+        @pl.when(s < k)
+        def _():
+            arrive_and_pass(k, 0)
 
     heads = attn[...]
     heads = heads * lax.rsqrt(jnp.mean(heads * heads, axis=-1, keepdims=True) + epsilon)
@@ -324,7 +331,7 @@
         jnp.ones((8, cols), f32), joined * joined, (((1,), (1,)), ((), ())),
         precision=highest, preferred_element_type=f32,
     )
-    y_all[s, t] = (joined * ffn_gain[:, columns(t)].astype(f32)).astype(bf16)
+    y_all[s, t] = (joined * ffn_gain[columns(t)].astype(f32).reshape(1, cols)).astype(bf16)
 
     def square_copy(j):
         return send(
@@ -335,31 +342,9 @@
     def total_copy(k):
         return send(total.at[0], total.at[k], total_send.at[k - 1], total_recv.at[k - 1], sp=up_by(k))
 
-    def up_y(k):
-        held_y = y_all.at[down_by(k - 1), t]
-        return send(held_y, held_y, up_send.at[k - 1], up_recv.at[k - 1], sp=lax.rem(s + 1, places))
-
-    def down_y(k):
-        held_y = y_all.at[up_by(k - 1), t]
-        return send(
-            held_y, held_y, down_send.at[k - 1], down_recv.at[k - 1], sp=lax.rem(s + places - 1, places)
-        )
-
-    def pass_up(k, finish=False):
-        @pl.when(jnp.logical_and(s + 1 < places, s >= k - 1))
-        def _():
-            if finish:
-                up_y(k).wait_send()
-            else:
-                up_y(k).start()
-
-    def pass_down(k, finish=False):
-        @pl.when(jnp.logical_and(s >= 1, s + k - 1 < places))
-        def _():
-            if finish:
-                down_y(k).wait_send()
-            else:
-                down_y(k).start()
+    def line_y(k):
+        mine = y_all.at[s, t]
+        return send(mine, mine, line_y_send.at[k - 1], line_y_recv.at[k - 1], sp=up_by(k))
 
     half = shares // 2
     near = t + 1 - 2 * lax.rem(t, 2)
@@ -380,14 +365,18 @@
 
     for j in range(1, shares):
         square_copy(j).start()
-    pass_up(1)
-    pass_down(1)
+    for k in far_first:
+        line_y(k).start()
     chip_y(0).start()
     core_y(0).start()
+    for k in far_first:
+        wide_start(k, 2)
     for k in range(1, places):
-        wide_start(far_first[k - 1], 2)
-    for k in range(1, places):
-        arrive_and_pass(k, 0)
+
+        @pl.when(s >= k)
+        def _():
+            arrive_and_pass(k, 0)
+
     squares = square_own[...]
     for j in range(1, shares):
         square_copy(j).wait_recv()
@@ -403,17 +392,13 @@
 
         @pl.when(s >= k)
         def _():
-            up_y(k).wait_recv()
-            if k + 1 < places:
-                pass_up(k + 1)
+            line_y(k).wait_recv()
             chip_y(k).start()
             core_y(k).start()
 
         @pl.when(s + k < places)
         def _():
-            down_y(k).wait_recv()
-            if k + 1 < places:
-                pass_down(k + 1)
+            line_y(places - k).wait_recv()
             chip_y(places - k).start()
             core_y(places - k).start()
 
@@ -504,8 +489,7 @@
     for k in range(1, places):
         for m in range(3):
             wide_sent(k, m)
-        pass_up(k, True)
-        pass_down(k, True)
+        line_y(k).wait_send()
         total_copy(k).wait_send()
         sum_copy(k).wait_send()
     for m in range(3):
@@ -545,7 +529,7 @@
     far = places - 1
     counts = [(4,)]
     for count in (
-        (far, 3), (copies - 1, far, 3), (HV // 128,), (shares - 1,), (shares - 1,), (far,), (far,), (far,),
+        (far, 3), (copies - 1, far, 3), (HV // 128,), (shares - 1,), (shares - 1,), (far,), (far,),
         (places,), (places,), (places,), (places,), (places,), (places,),
     ):
         counts += [count, count]
@@ -562,7 +546,7 @@
         ),
     )(
         stream, queries, key_matrix, value_matrix, output_gate_logits, forgetting_raw_score,
-        additional_forgetting_rate, head_norm_gain.reshape(1, -1), feedforward_norm_gain.reshape(1, -1),
+        additional_forgetting_rate, head_norm_gain.reshape(1, -1), feedforward_norm_gain,
         output_weight, gate_weight, up_weight, down_weight,
     )
 

time: 110 us -> 104 us (0.945)
  Pallas kernels: 107 us -> 102 us
  local copies, waits for them, and re-layouts: 2.86 us -> 1.57 us
    pallas_call x1, Pallas kernels: 107 us -> 102 us  [fused(): pl.pallas_call(kernel, out_shape=jax.ShapeDtypeStruct((tokens, cols), bf1...]
    reshape x1 -> x0, local copies, waits for them, and re-layouts: 1.29 us -> none  [fused(): feedforward_norm_gain.reshape(1, -1)]
where the time goes in v4:
time: 104 us
  Pallas kernels  102 us (98%)
  local copies, waits for them, and re-layouts  1.57 us (2%)
    pallas_call x1, Pallas kernels, fused(): pl.pallas_call(kernel, out_shape=jax.ShapeDtypeStruct((tokens, cols), bf1...  102 us

profile of v4, /device:TPU:0, one launch (start us, length us, event | category | flops | bytes accessed | tf_op | source)
XLA Modules:
  0.0 103.7 jit_solution(5013409561609672066)
XLA Ops:
  0.0 102.2 %shard_map.127 = bf16[128,512]{1,0:T(8,128)(2,1)} custom-call(bf16[128,2048]{1,0:T(8,128)(2,1)} %stream.1, bf16[128,256]{1,0:T(8,128)(2,1)} %queries.1, bf16[128,256]{1,0:T(8,128)(2,1)} %keys.1, bf16[128,512]{1,0:T(8,128)(2,1)} %values.1, bf16[128,512]{1,0:T(8,128)(2,1)} %out_gate.1, f32[128,256]{1,0:T(8,128)} %raw_score.1, f32[128,256]{1,0:T(8,128)} %extra_rate.1, ...), custom_call_target="tpu_custom_call" | custom-call | tf_op jit(solution)/shard_map/pallas_call | solution.py:537
  102.2 1.6 %copy.15 = bf16[128,512]{1,0:T(8,128)(2,1)} copy(bf16[128,512]{1,0:T(8,128)(2,1)} %shard_map.127) | data formatting | bytes 262144
